TPU v7x, 32 devices: a whole 2x2x4 slice. The times are simulated.
32 devices in a mesh: sp: 8 (over z, x), tp: 4 (over y, core).
Axes of the slice: x: 2, y: 2, z: 4, core: 2. Of those that a mesh axis runs over, the one named last changes fastest.
Arguments:
- layer_input: bfloat16 [8, 1536, 2048], P('sp', 'tp'), may hold values from -6 to 6
- input_gain: float32 [2048], replicated, may hold values from 0.1 to 1.9
- key_weight: bfloat16 [2048, 512], P('sp', 'tp'), may hold values from -0.125 to 0.125
- value_weight: bfloat16 [2048, 512], P('sp', 'tp'), may hold values from -0.125 to 0.125
- key_gain: float32 [128], replicated, may hold values from 0.1 to 1.9
- stop_shift: bfloat16 [8, 4, 1536], P('sp', None, 'tp'), may hold values from -20 to 0
- new_query: bfloat16 [8, 16, 128], P('sp', 'tp'), may hold values from -6 to 6
- query_gain: float32 [128], replicated, may hold values from 0.1 to 1.9
- out_gain: float32 [128], replicated, may hold values from 0.1 to 1.9
Outputs:
- key_cache: bfloat16 [8, 4, 1536, 128], P('sp', 'tp')
- value_cache: bfloat16 [8, 4, 1536, 128], P('sp', 'tp')
- shift_cache: bfloat16 [8, 4, 1536], P('sp', 'tp')
- first_read: bfloat16 [8, 16, 128], P('sp', 'tp')
All inputs are finite; a program needn't handle non-finite values.
Results may differ from a plain program's by a relative error of at most 0.013.
Values may be sent and summed in bfloat16 or wider, within the bound.
A program may use at most 64 MiB of HBM per device.

v0:
```python
import jax
import jax.numpy as jnp
from jax import lax
from jax.sharding import PartitionSpec as P

KVH = 4
epsilon = 1e-06


def row_norm(value_entries, scaling):
    return (
        value_entries
        * lax.rsqrt(jnp.mean(value_entries * value_entries, axis=-1, keepdims=True) + epsilon)
        * scaling
    )


def shards(
    layer_input,
    input_gain,
    key_weight,
    value_weight,
    key_gain,
    stop_shift,
    new_query,
    query_gain,
    out_gain,
):
    groups = lax.axis_size("tp")
    copies = groups // KVH
    row_count = layer_input.shape[1]
    head_size = new_query.shape[2]
    score_scale = 1.0 / head_size**0.5
    normed = row_norm(layer_input[0].astype(jnp.float32), input_gain).astype(jnp.bfloat16)
    stacked = jnp.stack((key_weight, value_weight), 0)
    full_depth = lax.all_gather(stacked, "sp", axis=1, tiled=True)
    projected = jnp.einsum(
        "rd,kdc->krc",
        normed,
        lax.all_gather(full_depth, "tp", axis=2, tiled=True),
        preferred_element_type=jnp.float32,
    )
    key_rows = row_norm(projected[0].reshape(row_count, KVH, head_size), key_gain).astype(
        jnp.bfloat16
    )
    value_rows = projected[1].reshape(row_count, KVH, head_size).astype(jnp.bfloat16)
    local_shift = stop_shift[0]
    key_slots = jnp.repeat(key_rows, copies, axis=1)
    value_slots = jnp.repeat(value_rows, copies, axis=1)
    shift_slots = jnp.repeat(local_shift.T, copies, axis=1)
    key_got, value_got, shift_got = (
        lax.all_to_all(key_slots, "tp", split_axis=1, concat_axis=0, tiled=True),
        lax.all_to_all(value_slots, "tp", split_axis=1, concat_axis=0, tiled=True),
        lax.all_to_all(shift_slots, "tp", split_axis=1, concat_axis=0, tiled=True),
    )
    key_line = key_got[:, 0, :]
    value_line = value_got[:, 0, :]
    shift_line = shift_got[:, 0]
    length = key_line.shape[0]
    query_rows = row_norm(new_query[0].astype(jnp.float32), query_gain).astype(jnp.bfloat16)
    scores = (
        jnp.einsum("qd,ld->ql", query_rows, key_line, preferred_element_type=jnp.float32)
        * score_scale
    )
    scores = scores + shift_line.astype(jnp.float32)[None, :]
    log_keep = jax.nn.log_sigmoid(-scores)
    inside = lax.cumsum(log_keep, axis=1, reverse=True) - log_keep
    weights = jnp.exp(jax.nn.log_sigmoid(scores) + inside).astype(jnp.bfloat16)
    read_sum = jnp.dot(weights, value_line, preferred_element_type=jnp.float32)
    first_out = row_norm(read_sum, out_gain).astype(jnp.bfloat16)
    return (
        key_line.reshape(1, 1, length, head_size),
        value_line.reshape(1, 1, length, head_size),
        shift_line.reshape(1, 1, length),
        first_out[None],
    )


def solution(mesh):
    placed = (
        P("sp", "tp", None),
        P(),
        P("sp", "tp"),
        P("sp", "tp"),
        P(),
        P("sp", None, "tp"),
        P("sp", "tp", None),
        P(),
        P(),
    )
    return jax.shard_map(
        shards,
        mesh=mesh,
        in_specs=placed,
        out_specs=(
            P("sp", "tp", None, None),
            P("sp", "tp", None, None),
            P("sp", "tp", None),
            P("sp", "tp", None),
        ),
        check_vma=False,
    )
```

profile of v0, /device:TPU:0, one launch (start us, length us, event | category | flops | bytes accessed | tf_op | source)
XLA Modules:
  0.0 125.1 jit_solution(7521093562815016131)
XLA Ops:
  7.2 1.0 copy.25
  8.3 0.9 copy.26
  9.2 0.7 pad_maximum_fusion
  10.0 42.8 %all-gather.3.cloned.1.call-done = bf16[2,2048,128]{1,2,0:T(8,128)(2,1)} async-done(((bf16[2,256,128]{1,2,0:T(8,128)(2,1)}), bf16[2,2048,128]{1,2,0:T(8,128)(2,1)}) %all-gather.3.cloned.1.call-update) | async-done | bytes 1048592 | tf_op jit(solution)/shard_map/all_gather | solution.py:36
  52.8 0.7 copy.36
  53.5 0.5 broadcast.75
  54.0 0.7 reduce.5
  54.7 0.7 reshape.96
  55.3 3.2 %all-to-all-start.2 = ((bf16[4,2,192]{2,1,0:T(2,128)(2,1)}), bf16[4,2,192]{2,1,0:T(2,128)(2,1)S(1)}, u32[]{:S(2)}, u32[]{:S(2)}) async-start(bf16[4,2,192]{2,1,0:T(2,128)(2,1)} %reshape.96), calls=%async_computation.2 | async-start | bytes 8192 | tf_op jit(solution)/shard_map/all_to_all | solution.py:54
  58.6 0.8 fusion.22
  59.4 1.9 %fusion = f32[384]{0:T(512)S(1)} fusion(bf16[1,384,2048]{2,1,0:T(8,128)(2,1)} %param.9), kind=kLoop, calls=%fused_computation.2 | loop fusion | flops 2358912 | bytes 1574400 | tf_op jit(solution)/shard_map/reduce_sum | solution.py:13
  61.4 26.5 %all-gather.5.cloned.1.call-done = bf16[2,2048,512]{1,2,0:T(8,128)(2,1)} async-done(((bf16[2,2048,128]{1,2,0:T(8,128)(2,1)}), bf16[2,2048,512]{1,2,0:T(8,128)(2,1)}) %all-gather.5.cloned.1.call-update) | async-done | bytes 4194320 | tf_op jit(solution)/shard_map/all_gather | solution.py:40
  87.8 4.6 %fusion.10 = f32[2,384,512]{1,2,0:T(8,128)S(1)} fusion(bf16[2,2048,512]{1,2,0:T(8,128)(2,1)} %all-gather.5.cloned.1.call-done, bf16[1,384,2048]{2,1,0:T(8,128)(2,1)S(1)} %copy-done, f32[2048]{0:T(1024)S(1)} %copy-done.6, f32[384]{0:T(512)S(1)} %add_rsqrt_fusion.1), kind=kOutput, calls=%fused_computation.12 | convolution fusion | flops 1613758464 | bytes 7349760 | tf_op jit(solution)/shard_map/rd,kdc->krc/dot_general | solution.py:37
  93.1 1.0 multiply_convert_fusion
  94.1 3.5 %all-to-all-start = ((bf16[384,4,128]{2,0,1:T(8,128)(2,1)}), bf16[384,4,128]{2,0,1:T(8,128)(2,1)S(1)}, u32[]{:S(2)}, u32[]{:S(2)}) async-start(bf16[384,4,128]{2,0,1:T(8,128)(2,1)} %multiply_convert_fusion), calls=%async_computation | async-start | bytes 786432 | tf_op jit(solution)/shard_map/all_to_all | solution.py:52
  97.8 0.9 copy.28
  98.7 6.3 %all-to-all-done = bf16[384,4,128]{2,0,1:T(8,128)(2,1)S(1)} async-done(((bf16[384,4,128]{2,0,1:T(8,128)(2,1)}), bf16[384,4,128]{2,0,1:T(8,128)(2,1)S(1)}, u32[]{:S(2)}, u32[]{:S(2)}) %all-to-all-start) | async-done | bytes 393248 | tf_op jit(solution)/shard_map/all_to_all | solution.py:52
  105.0 3.5 %all-to-all-start.1 = ((bf16[384,4,128]{2,0,1:T(8,128)(2,1)}), bf16[384,4,128]{2,0,1:T(8,128)(2,1)S(1)}, u32[]{:S(2)}, u32[]{:S(2)}) async-start(bf16[384,4,128]{2,0,1:T(8,128)(2,1)} %copy.28), calls=%async_computation.1 | async-start | bytes 786432 | tf_op jit(solution)/shard_map/all_to_all | solution.py:53
  108.8 5.0 %reduce-window.6 = f32[4,12,128]{2,1,0:T(8,128)S(1)} reduce-window(f32[4,12,128]{2,1,0:T(8,128)S(1)} %reshape.89, f32[]{:T(128)} %constant.8.clone.1), window={size=1x1x128 pad=0_0x0_0x0_127}, to_apply=%region_3.4 | reduce-window | flops 780288 | bytes 49156 | tf_op jit(solution)/shard_map/reduce-window
  114.2 1.6 %all-to-all-done.1 = bf16[384,4,128]{2,0,1:T(8,128)(2,1)S(1)} async-done(((bf16[384,4,128]{2,0,1:T(8,128)(2,1)}), bf16[384,4,128]{2,0,1:T(8,128)(2,1)S(1)}, u32[]{:S(2)}, u32[]{:S(2)}) %all-to-all-start.1) | async-done | bytes 393248 | tf_op jit(solution)/shard_map/all_to_all | solution.py:53
  115.8 0.3 multiply_reduce_fusion.1
  116.2 0.6 fusion.25
  116.8 0.7 copy.39
  117.5 0.7 copy.40
  (36 shorter events, 1.6 us)
Async XLA Ops:
  7.2 80.7 %copy-start = (bf16[1,384,2048]{2,1,0:T(8,128)(2,1)S(1)}, bf16[1,384,2048]{2,1,0:T(8,128)(2,1)}, u32[]{:S(2)}) copy-start(bf16[1,384,2048]{2,1,0:T(8,128)(2,1)} %param.9) | copy-start | bytes 4718596
  7.2 80.7 %copy-start.6 = (f32[2048]{0:T(1024)S(1)}, f32[2048]{0:T(1024)}, u32[]{:S(2)}) copy-start(f32[2048]{0:T(1024)} %param.10) | copy-start | bytes 24580
  7.2 45.6 %all-gather.3.cloned.1.call-start = ((), (), s32[]{:S(2)}) async-start(), calls=%async_computation.3 | async-start | bytes 1179648 | tf_op jit(solution)/shard_map/all_gather | solution.py:36
  9.9 77.9 %all-gather.5.cloned.1.call-start = ((), (), s32[]{:S(2)}) async-start(), calls=%async_computation.4 | async-start | bytes 5242880 | tf_op jit(solution)/shard_map/all_gather | solution.py:40
  55.3 38.8 %all-to-all-start.2 = ((bf16[4,2,192]{2,1,0:T(2,128)(2,1)}), bf16[4,2,192]{2,1,0:T(2,128)(2,1)S(1)}, u32[]{:S(2)}, u32[]{:S(2)}) async-start(bf16[4,2,192]{2,1,0:T(2,128)(2,1)} %reshape.96), calls=%async_computation.2 | async-start | bytes 8192 | tf_op jit(solution)/shard_map/all_to_all | solution.py:54
  92.5 0.7 copy-start.3
  92.5 15.9 %copy-start.2 = (bf16[1,4,128]{2,1,0:T(4,128)(2,1)S(1)}, bf16[1,4,128]{2,1,0:T(4,128)(2,1)}, u32[]{:S(2)}) copy-start(bf16[1,4,128]{2,1,0:T(4,128)(2,1)} %param.15) | copy-start | bytes 3076
  92.5 15.9 %copy-start.4 = (f32[128]{0:T(128)S(1)}, f32[128]{0:T(128)}, u32[]{:S(2)}) copy-start(f32[128]{0:T(128)} %param.16) | copy-start | bytes 1540
  92.8 23.3 %copy-start.5 = (f32[128]{0:T(128)S(1)}, f32[128]{0:T(128)}, u32[]{:S(2)}) copy-start(f32[128]{0:T(128)} %param.17) | copy-start | bytes 1540
  94.1 10.8 %all-to-all-start = ((bf16[384,4,128]{2,0,1:T(8,128)(2,1)}), bf16[384,4,128]{2,0,1:T(8,128)(2,1)S(1)}, u32[]{:S(2)}, u32[]{:S(2)}) async-start(bf16[384,4,128]{2,0,1:T(8,128)(2,1)} %multiply_convert_fusion), calls=%async_computation | async-start | bytes 786432 | tf_op jit(solution)/shard_map/all_to_all | solution.py:52
  97.7 20.6 %copy-start.1 = (bf16[4,1,384]{2,1,0:T(2,128)(2,1)}, bf16[4,1,384]{2,1,0:T(2,128)(2,1)S(1)}, u32[]{:S(2)}) copy-start(bf16[4,1,384]{2,1,0:T(2,128)(2,1)S(1)} %reshape.97) | copy-start | bytes 9220
  105.0 10.8 %all-to-all-start.1 = ((bf16[384,4,128]{2,0,1:T(8,128)(2,1)}), bf16[384,4,128]{2,0,1:T(8,128)(2,1)S(1)}, u32[]{:S(2)}, u32[]{:S(2)}) async-start(bf16[384,4,128]{2,0,1:T(8,128)(2,1)} %copy.28), calls=%async_computation.1 | async-start | bytes 786432 | tf_op jit(solution)/shard_map/all_to_all | solution.py:53
Sparse Core Ops, SparseCore 0:
  10.6 42.1 all-gather.2
  54.3 33.4 all-gather.4
where the time goes:
time: 126 us; the launch traced here: 125 us
  waiting for transfers between devices  77.2 us (61%)
  between operations  14.2 us (11%)
  other arithmetic  11.1 us (9%)
  starting transfers between devices  10.2 us (8%)
  local copies, waits for them, and re-layouts  7.15 us (6%)
  matrix products  5.2 us (4%)
    all_gather x1, waiting for transfers between devices, shards(): full_depth = lax.all_gather(stacked, 'sp', axis=1, tiled=True)  42.8 us
    all_gather x1, waiting for transfers between devices, shards(): lax.all_gather(full_depth, 'tp', axis=2, tiled=True)  26.5 us
    all_to_all x1, waiting for transfers between devices, shards(): lax.all_to_all(key_slots, 'tp', split_axis=1, concat_axis=0, tiled=True)  6.25 us
    another operation x2, other arithmetic  5.17 us
    unnamed x21, local copies, waits for them, and re-layouts  4.98 us
    dot_general x1, matrix products, shards(): jnp.einsum('rd,kdc->krc', normed, lax.all_gather(full_depth, 'tp', axis=2...  4.62 us
    all_to_all x1, starting transfers between devices, shards(): lax.all_to_all(key_slots, 'tp', split_axis=1, concat_axis=0, tiled=True)  3.46 us
    all_to_all x1, starting transfers between devices, shards(): lax.all_to_all(value_slots, 'tp', split_axis=1, concat_axis=0, tiled=True)  3.46 us
  transfers between devices with their start and end apart: 5, of which 4 were waited for; matrix products, arithmetic and copies ran while one was open for 14% of the time, Pallas kernels for 0%

commit v1 on v0

--- a/solution.py
+++ b/solution.py
@@ -5,6 +5,27 @@
 
 KVH = 4
 epsilon = 1e-06
+
+
+def laid_out(parts, dim):
+    parts = jnp.moveaxis(parts, 0, dim)
+    shape = parts.shape
+    return parts.reshape(*shape[:dim], shape[dim] * shape[dim + 1], *shape[dim + 2 :])
+
+
+def grow_blocks(x, axis):
+    size, here = (lax.axis_size(axis), lax.axis_index(axis))
+    blocks, bit = (x[None], 1)
+    while bit < size:
+        other = lax.ppermute(blocks, axis, [(i, i ^ bit) for i in range(size)])
+        low = here & bit == 0
+        blocks = jnp.concatenate([jnp.where(low, blocks, other), jnp.where(low, other, blocks)])
+        bit *= 2
+    return blocks
+
+
+def doubled_up(x, axis, dim):
+    return laid_out(grow_blocks(x, axis), dim)
 
 
 def row_norm(value_entries, scaling):
@@ -35,10 +56,7 @@
     stacked = jnp.stack((key_weight, value_weight), 0)
     full_depth = lax.all_gather(stacked, "sp", axis=1, tiled=True)
     projected = jnp.einsum(
-        "rd,kdc->krc",
-        normed,
-        lax.all_gather(full_depth, "tp", axis=2, tiled=True),
-        preferred_element_type=jnp.float32,
+        "rd,kdc->krc", normed, doubled_up(full_depth, "tp", 2), preferred_element_type=jnp.float32
     )
     key_rows = row_norm(projected[0].reshape(row_count, KVH, head_size), key_gain).astype(
         jnp.bfloat16

time: 126 us -> 156 us (1.24)
  waiting for transfers between devices: 77.2 us -> 95.2 us
  other arithmetic: 11.1 us -> 18.2 us
  local copies, waits for them, and re-layouts: 7.15 us -> 11 us
  starting transfers between devices: 10.2 us -> 11.8 us
    ppermute x0 -> x2, waiting for transfers between devices: none -> 42.3 us  [grow_blocks(): other = lax.ppermute(blocks, axis, [(i, i ^ bit) for i in range(size)])]
    all_gather x1 -> x0, waiting for transfers between devices: 26.5 us -> none  [shards(): lax.all_gather(full_depth, 'tp', axis=2, tiled=True)]
    transpose x0 -> x1, local copies, waits for them, and re-layouts: none -> 6.51 us  [laid_out(): parts = jnp.moveaxis(parts, 0, dim)]
    select_n x0 -> x2, other arithmetic: none -> 3.23 us  [grow_blocks(): jnp.where(low, blocks, other)]
    transpose x0 -> x1, other arithmetic: none -> 2.29 us  [laid_out(): parts = jnp.moveaxis(parts, 0, dim)]
    all_gather x1, waiting for transfers between devices: 42.8 us -> 45 us  [shards(): full_depth = lax.all_gather(stacked, 'sp', axis=1, tiled=True)]
    unnamed x21, local copies, waits for them, and re-layouts: 4.98 us -> 3.03 us
  transfers between devices with their start and end apart: 5 -> 6, of which waited for: 4 -> 5; matrix products, arithmetic and copies ran while one was open for 14% -> 18% of each run, Pallas kernels for 0% -> 0%
where the time goes in v1:
time: 156 us
  waiting for transfers between devices  95.2 us (61%)
  other arithmetic  18.2 us (12%)
  between operations  14.2 us (9%)
  starting transfers between devices  11.8 us (8%)
  local copies, waits for them, and re-layouts  11 us (7%)
  matrix products  5.2 us (3%)
    all_gather x1, waiting for transfers between devices, shards(): full_depth = lax.all_gather(stacked, 'sp', axis=1, tiled=True)  45 us
    ppermute x2, waiting for transfers between devices, grow_blocks(): other = lax.ppermute(blocks, axis, [(i, i ^ bit) for i in range(size)])  42.3 us
    transpose x1, local copies, waits for them, and re-layouts, laid_out(): parts = jnp.moveaxis(parts, 0, dim)  6.51 us
    all_to_all x1, waiting for transfers between devices, shards(): lax.all_to_all(key_slots, 'tp', split_axis=1, concat_axis=0, tiled=True)  6.25 us
    another operation x2, other arithmetic  5.17 us
    dot_general x1, matrix products, shards(): jnp.einsum('rd,kdc->krc', normed, doubled_up(full_depth, 'tp', 2), prefer...  4.62 us
    all_to_all x1, starting transfers between devices, shards(): lax.all_to_all(key_slots, 'tp', split_axis=1, concat_axis=0, tiled=True)  3.59 us
    all_to_all x1, starting transfers between devices, shards(): lax.all_to_all(value_slots, 'tp', split_axis=1, concat_axis=0, tiled=True)  3.46 us
  transfers between devices with their start and end apart: 6, of which 5 were waited for; matrix products, arithmetic and copies ran while one was open for 18% of the time, Pallas kernels for 0%

profile of v1, /device:TPU:0, one launch (start us, length us, event | category | flops | bytes accessed | tf_op | source)
XLA Modules:
  0.0 155.7 jit_solution(16078421419363230683)
XLA Ops:
  7.2 1.5 pad_maximum_fusion.1
  8.8 45.0 %all-gather.2.cloned.1.call-done = bf16[2,2048,128]{2,1,0:T(8,128)(2,1)} async-done(((bf16[2,256,128]{2,1,0:T(8,128)(2,1)}), bf16[2,2048,128]{2,1,0:T(8,128)(2,1)}) %all-gather.2.cloned.1.call-update) | async-done | bytes 1048592 | tf_op jit(solution)/shard_map/all_gather | solution.py:57
  53.7 2.9 %collective-permute-done = bf16[1,2,2048,128]{3,2,1,0:T(8,128)(2,1)S(1)} collective-permute-done((bf16[1,2,2048,128]{3,2,1,0:T(8,128)(2,1)}, bf16[1,2,2048,128]{3,2,1,0:T(8,128)(2,1)S(1)}, u32[]{:S(2)}, u32[]{:S(2)}) %collective-permute-start) | collective-permute-done | bytes 1048608 | tf_op jit(solution)/shard_map/ppermute | solution.py:20
  56.6 1.4 broadcast_select_fusion.3
  58.0 1.5 pad_maximum_fusion
  59.5 1.5 collective-permute-start.1
  61.5 0.7 reduce.6
  62.2 0.7 reshape.113
  62.9 3.2 %all-to-all-start.2 = ((bf16[4,2,192]{2,1,0:T(2,128)(2,1)}), bf16[4,2,192]{2,1,0:T(2,128)(2,1)S(1)}, u32[]{:S(2)}, u32[]{:S(2)}) async-start(bf16[4,2,192]{2,1,0:T(2,128)(2,1)} %reshape.113), calls=%async_computation.2 | async-start | bytes 8192 | tf_op jit(solution)/shard_map/all_to_all | solution.py:72
  66.3 1.8 %fusion = f32[384]{0:T(512)S(1)} fusion(bf16[1,384,2048]{2,1,0:T(8,128)(2,1)} %param.9), kind=kLoop, calls=%fused_computation.3 | loop fusion | flops 2358912 | bytes 1574400 | tf_op jit(solution)/shard_map/reduce_sum | solution.py:34
  68.1 39.5 %collective-permute-done.1 = bf16[2,2,2048,128]{3,2,1,0:T(8,128)(2,1)} collective-permute-done((bf16[2,2,2048,128]{3,2,1,0:T(8,128)(2,1)}, bf16[2,2,2048,128]{3,2,1,0:T(8,128)(2,1)}, u32[]{:S(2)}, u32[]{:S(2)}) %collective-permute-start.1) | collective-permute-done | bytes 2097184 | tf_op jit(solution)/shard_map/ppermute | solution.py:20
  107.5 1.9 %broadcast_select_fusion.1 = (bf16[2,2,2048,128]{3,2,1,0:T(8,128)(2,1)S(1)}, bf16[2,2,2048,128]{3,2,1,0:T(8,128)(2,1)S(1)}) fusion(bf16[2,2,2048,128]{3,2,1,0:T(8,128)(2,1)} %collective-permute-done.1, pred[]{:T(512)S(6)} %eq.6, bf16[1,2,2048,128]{3,2,1,0:T(8,128)(2,1)S(1)} %get-tuple-element.7, bf16[1,2,2048,128]{3,2,1,0:T(8,128)(2,1)S(1)} %get-tuple-element.6), kind=kLoop, calls=%fused_computation.10 | loop fusion | flops 3145728 | bytes 8388609 | tf_op jit(solution)/shard_map/jit(_where)/select_n | solution.py:22
  109.4 2.3 %maximum_bitcast_fusion = bf16[2,2048,4,128]{3,1,0,2:T(8,128)(2,1)} fusion(bf16[2,2,2048,128]{3,2,1,0:T(8,128)(2,1)S(1)} %get-tuple-element.5, bf16[2,2,2048,128]{3,2,1,0:T(8,128)(2,1)S(1)} %get-tuple-element.4), kind=kLoop, calls=%fused_computation | loop fusion | flops 2097152 | bytes 8388608 | tf_op jit(solution)/shard_map/transpose | solution.py:11
  111.7 6.5 %copy.22 = bf16[2,2048,4,128]{1,3,2,0:T(8,128)(2,1)} copy(bf16[2,2048,4,128]{3,1,0,2:T(8,128)(2,1)} %maximum_bitcast_fusion) | data formatting | bytes 8388608 | tf_op jit(solution)/shard_map/transpose | solution.py:11
  118.2 4.6 %fusion.9 = f32[2,384,512]{1,2,0:T(8,128)S(1)} fusion(bf16[2,2048,512]{1,2,0:T(8,128)(2,1)} %bitcast.69, bf16[1,384,2048]{2,1,0:T(8,128)(2,1)S(1)} %copy-done, f32[2048]{0:T(1024)S(1)} %copy-done.7, f32[384]{0:T(512)S(1)} %add_rsqrt_fusion.1), kind=kOutput, calls=%fused_computation.15 | convolution fusion | flops 1613758464 | bytes 7349760 | tf_op jit(solution)/shard_map/rd,kdc->krc/dot_general | solution.py:58
  123.5 1.0 multiply_convert_fusion
  124.5 3.6 %all-to-all-start = ((bf16[384,4,128]{2,0,1:T(8,128)(2,1)}), bf16[384,4,128]{2,0,1:T(8,128)(2,1)S(1)}, u32[]{:S(2)}, u32[]{:S(2)}) async-start(bf16[384,4,128]{2,0,1:T(8,128)(2,1)} %multiply_convert_fusion), calls=%async_computation | async-start | bytes 786432 | tf_op jit(solution)/shard_map/all_to_all | solution.py:70
  128.3 0.9 copy.24
  129.3 6.3 %all-to-all-done = bf16[384,4,128]{2,0,1:T(8,128)(2,1)S(1)} async-done(((bf16[384,4,128]{2,0,1:T(8,128)(2,1)}), bf16[384,4,128]{2,0,1:T(8,128)(2,1)S(1)}, u32[]{:S(2)}, u32[]{:S(2)}) %all-to-all-start) | async-done | bytes 393248 | tf_op jit(solution)/shard_map/all_to_all | solution.py:70
  135.5 3.5 %all-to-all-start.1 = ((bf16[384,4,128]{2,0,1:T(8,128)(2,1)}), bf16[384,4,128]{2,0,1:T(8,128)(2,1)S(1)}, u32[]{:S(2)}, u32[]{:S(2)}) async-start(bf16[384,4,128]{2,0,1:T(8,128)(2,1)} %copy.24), calls=%async_computation.1 | async-start | bytes 786432 | tf_op jit(solution)/shard_map/all_to_all | solution.py:71
  139.3 5.0 %reduce-window.6 = f32[4,12,128]{2,1,0:T(8,128)S(1)} reduce-window(f32[4,12,128]{2,1,0:T(8,128)S(1)} %reshape.107, f32[]{:T(128)} %constant.13.clone.1), window={size=1x1x128 pad=0_0x0_0x0_127}, to_apply=%region_3.4 | reduce-window | flops 780288 | bytes 49156 | tf_op jit(solution)/shard_map/reduce-window
  144.7 1.7 %all-to-all-done.1 = bf16[384,4,128]{2,0,1:T(8,128)(2,1)S(1)} async-done(((bf16[384,4,128]{2,0,1:T(8,128)(2,1)}), bf16[384,4,128]{2,0,1:T(8,128)(2,1)S(1)}, u32[]{:S(2)}, u32[]{:S(2)}) %all-to-all-start.1) | async-done | bytes 393248 | tf_op jit(solution)/shard_map/all_to_all | solution.py:71
  147.3 0.7 copy.35
  148.1 0.7 copy.36
  (42 shorter events, 3.2 us)
Async XLA Ops:
  7.2 46.6 %all-gather.2.cloned.1.call-start = ((), (), s32[]{:S(2)}) async-start(), calls=%async_computation.3 | async-start | bytes 1179648 | tf_op jit(solution)/shard_map/all_gather | solution.py:57
  53.7 2.9 %collective-permute-start = (bf16[1,2,2048,128]{3,2,1,0:T(8,128)(2,1)}, bf16[1,2,2048,128]{3,2,1,0:T(8,128)(2,1)S(1)}, u32[]{:S(2)}, u32[]{:S(2)}) collective-permute-start(bf16[1,2,2048,128]{3,2,1,0:T(8,128)(2,1)} %bitcast.75), channel_id=1, source_target_pairs={{0,1},{1,0},{2,3},{3,2},{4,5},{5,4},{6,7},{7,6},{8,9},{9,8},{10,11... | collective-permute-start | bytes 3145736 | tf_op jit(solution)/shard_map/ppermute | solution.py:20
  58.0 3.0 %copy-start.2 = (bf16[1,4,384]{2,1,0:T(4,128)(2,1)S(1)}, bf16[1,4,384]{2,1,0:T(4,128)(2,1)}, u32[]{:S(2)}) copy-start(bf16[1,4,384]{2,1,0:T(4,128)(2,1)} %param.14) | copy-start | bytes 9220
  58.0 8.2 %copy-start.3 = (bf16[1,4,128]{2,1,0:T(4,128)(2,1)S(1)}, bf16[1,4,128]{2,1,0:T(4,128)(2,1)}, u32[]{:S(2)}) copy-start(bf16[1,4,128]{2,1,0:T(4,128)(2,1)} %param.15) | copy-start | bytes 3076
  59.5 48.0 %collective-permute-start.1 = (bf16[2,2,2048,128]{3,2,1,0:T(8,128)(2,1)}, bf16[2,2,2048,128]{3,2,1,0:T(8,128)(2,1)}, u32[]{:S(2)}, u32[]{:S(2)}) collective-permute-start(bf16[2,2,2048,128]{3,2,1,0:T(8,128)(2,1)} %pad_maximum_fusion), channel_id=1, source_target_pairs={{0,2},{1,3},{2,0},{3,1},{4,6},{5,7},{6,4},{7,5},{8,10},{9,11},{10,... | collective-permute-start | bytes 6291464 | tf_op jit(solution)/shard_map/ppermute | solution.py:20
  62.9 61.6 %all-to-all-start.2 = ((bf16[4,2,192]{2,1,0:T(2,128)(2,1)}), bf16[4,2,192]{2,1,0:T(2,128)(2,1)S(1)}, u32[]{:S(2)}, u32[]{:S(2)}) async-start(bf16[4,2,192]{2,1,0:T(2,128)(2,1)} %reshape.113), calls=%async_computation.2 | async-start | bytes 8192 | tf_op jit(solution)/shard_map/all_to_all | solution.py:72
  111.7 6.5 %copy-start = (bf16[1,384,2048]{2,1,0:T(8,128)(2,1)S(1)}, bf16[1,384,2048]{2,1,0:T(8,128)(2,1)}, u32[]{:S(2)}) copy-start(bf16[1,384,2048]{2,1,0:T(8,128)(2,1)} %param.9) | copy-start | bytes 4718596
  111.7 6.5 %copy-start.7 = (f32[2048]{0:T(1024)S(1)}, f32[2048]{0:T(1024)}, u32[]{:S(2)}) copy-start(f32[2048]{0:T(1024)} %param.10) | copy-start | bytes 24580
  122.8 0.7 copy-start.4
  123.5 15.5 %copy-start.5 = (f32[128]{0:T(128)S(1)}, f32[128]{0:T(128)}, u32[]{:S(2)}) copy-start(f32[128]{0:T(128)} %param.16) | copy-start | bytes 1540
  124.5 22.2 %copy-start.6 = (f32[128]{0:T(128)S(1)}, f32[128]{0:T(128)}, u32[]{:S(2)}) copy-start(f32[128]{0:T(128)} %param.17) | copy-start | bytes 1540
  124.5 11.0 %all-to-all-start = ((bf16[384,4,128]{2,0,1:T(8,128)(2,1)}), bf16[384,4,128]{2,0,1:T(8,128)(2,1)S(1)}, u32[]{:S(2)}, u32[]{:S(2)}) async-start(bf16[384,4,128]{2,0,1:T(8,128)(2,1)} %multiply_convert_fusion), calls=%async_computation | async-start | bytes 786432 | tf_op jit(solution)/shard_map/all_to_all | solution.py:70
  128.2 19.8 %copy-start.1 = (bf16[4,1,384]{2,1,0:T(2,128)(2,1)}, bf16[4,1,384]{2,1,0:T(2,128)(2,1)S(1)}, u32[]{:S(2)}) copy-start(bf16[4,1,384]{2,1,0:T(2,128)(2,1)S(1)} %reshape.114) | copy-start | bytes 9220
  135.5 10.8 %all-to-all-start.1 = ((bf16[384,4,128]{2,0,1:T(8,128)(2,1)}), bf16[384,4,128]{2,0,1:T(8,128)(2,1)S(1)}, u32[]{:S(2)}, u32[]{:S(2)}) async-start(bf16[384,4,128]{2,0,1:T(8,128)(2,1)} %copy.24), calls=%async_computation.1 | async-start | bytes 786432 | tf_op jit(solution)/shard_map/all_to_all | solution.py:71
Sparse Core Ops, SparseCore 0:
  10.7 42.9 all-gather.1
